TPU v7x, 32 devices: a whole 2x2x4 slice. The times are simulated.
32 devices in a mesh: grp: 2 (over y), tp: 4 (over z), dp: 4 (over x, core).
Axes of the slice: x: 2, y: 2, z: 4, core: 2. Of those that a mesh axis runs over, the one named last changes fastest.
Arguments:
- tokens: bfloat16 [128, 4096], P('grp', 'dp'), parts along dimension 0, may hold values from -6 to 6
- norm_gain: float32 [2, 4096], P(None, 'dp'), may hold values from 0.1 to 1.9
- w_query: bfloat16 [2, 4096, 512], P(None, 'dp', 'tp'), may hold values from -0.09375 to 0.09375
- w_key: bfloat16 [2, 4096, 512], P(None, 'dp', 'tp'), may hold values from -0.09375 to 0.09375
- w_value: bfloat16 [2, 4096, 512], P(None, 'dp', 'tp'), may hold values from -0.09375 to 0.09375
- w_outgate: bfloat16 [2, 4096, 512], P(None, 'dp', 'tp'), may hold values from -0.09375 to 0.09375
- gate_weight: bfloat16 [2, 4, 384, 2], P(None, 'tp'), may hold values from -0.3125 to 0.3125
- forget_bias: float32 [2, 4], P(None, 'tp'), may hold values from -2 to 4
- w_mix: bfloat16 [2, 512, 4096], P(None, 'tp', 'dp'), may hold values from -0.25 to 0.25
- memory: float32 [2, 128, 4, 128, 128], P(None, ('grp', 'dp'), 'tp'), parts along dimension 1, may hold values from -3 to 3
- normalizer: float32 [2, 128, 4, 128], P(None, ('grp', 'dp'), 'tp'), parts along dimension 1, may hold values from -3 to 3
- stabilizer: float32 [2, 128, 4], P(None, ('grp', 'dp'), 'tp'), parts along dimension 1, may hold values from -4 to 4
Outputs:
- result: bfloat16 [128, 4096], P('grp', 'dp'), parts along dimension 0
- new_memory: float32 [2, 128, 4, 128, 128], P(None, ('grp', 'dp'), 'tp'), parts along dimension 1
- new_normalizer: float32 [2, 128, 4, 128], P(None, ('grp', 'dp'), 'tp'), parts along dimension 1
- new_stabilizer: float32 [2, 128, 4], P(None, ('grp', 'dp'), 'tp'), parts along dimension 1
There are 2 independent parts, one for each index of `grp`. A program takes and returns all parts, laid end to end along the dimension named above; an argument that names none is the same for every part. Nothing has to cross between parts.
All inputs are finite; a program needn't handle non-finite values.
Results may differ from a plain program's by a relative error of at most 0.018.
Values may be sent and summed in bfloat16 or wider, within the bound.
A program may use at most 64 MiB of HBM per device.

v0:
```python
import jax
import jax.numpy as jnp
from jax import lax
from jax.sharding import PartitionSpec as P

D = 4096
DK = 128
BLOCKS = 2


EPS = 1e-06


def shards(
    tokens,
    norm_gain,
    w_query,
    w_key,
    w_value,
    w_outgate,
    gate_weight,
    forget_bias,
    w_mix,
    memory,
    normalizer,
    stabilizer,
):
    x = tokens
    seq_own = memory.shape[1]
    heads_own = memory.shape[2]
    mems, norms, stabs = ([], [], [])
    for blk in range(BLOCKS):
        xf = x.astype(jnp.float32)
        squares = jnp.sum(xf * xf, axis=-1)
        scaled_in = (xf * norm_gain[blk]).astype(jnp.bfloat16)
        terms = tuple(
            (
                jnp.dot(scaled_in, weight[blk], preferred_element_type=jnp.float32)
                for weight in (w_query, w_key, w_value, w_outgate)
            )
        )
        totals = lax.psum(squares, "dp")
        summed = lax.psum_scatter(terms, "dp", scatter_dimension=0, tiled=True)
        own_squares = lax.dynamic_slice_in_dim(totals, lax.axis_index("dp") * seq_own, seq_own, 0)
        scale = lax.rsqrt(own_squares / D + EPS)
        projs = [
            (scale[:, None] * part)
            .astype(jnp.bfloat16)
            .astype(jnp.float32)
            .reshape(seq_own, heads_own, DK)
            for part in summed
        ]
        query, key, value, outgate = projs
        joined = jnp.concatenate([query, key, value], axis=-1)
        pre = jnp.einsum(
            "shc,hcg->shg",
            joined,
            gate_weight[blk].astype(jnp.float32),
            precision=lax.Precision.HIGHEST,
        )
        log_input = pre[..., 0]
        log_forget = jax.nn.log_sigmoid(pre[..., 1] + forget_bias[blk])
        stab = stabilizer[blk]
        new_stab = jnp.maximum(log_forget + stab, log_input)
        keep = jnp.exp(log_forget + stab - new_stab)
        admit = jnp.exp(log_input - new_stab)
        scaled_key = key * DK ** (-0.5)
        new_mem = (
            keep[..., None, None] * memory[blk]
            + admit[..., None, None] * scaled_key[..., :, None] * value[..., None, :]
        )
        new_norm = keep[..., None] * normalizer[blk] + admit[..., None] * scaled_key
        numer = jnp.einsum("shd,shde->she", query, new_mem, precision=lax.Precision.HIGHEST)
        denom = jnp.maximum(jnp.abs(jnp.sum(query * new_norm, axis=-1)), 1.0)
        readout = numer / denom[..., None]
        gated = (
            (readout * jax.nn.sigmoid(outgate))
            .reshape(seq_own, heads_own * DK)
            .astype(jnp.bfloat16)
        )
        mix_weight = w_mix[blk]
        partial_mix = jnp.dot(
            lax.all_gather(gated, "dp", axis=0, tiled=True),
            mix_weight,
            preferred_element_type=jnp.float32,
        )
        mine = lax.psum_scatter(partial_mix, "tp", scatter_dimension=0, tiled=True)
        row_count = mine.shape[0]
        own_rows = lax.dynamic_slice_in_dim(xf, lax.axis_index("tp") * row_count, row_count, 0)
        updated = (own_rows + mine).astype(jnp.bfloat16)
        x = lax.all_gather(updated, "tp", axis=0, tiled=True)
        mems.append(new_mem)
        norms.append(new_norm)
        stabs.append(new_stab)
    return (x, jnp.stack(mems, axis=0), jnp.stack(norms, axis=0), jnp.stack(stabs, axis=0))


def solution(mesh):
    in_specs = (
        P("grp", "dp"),
        P(None, "dp"),
        P(None, "dp", "tp"),
        P(None, "dp", "tp"),
        P(None, "dp", "tp"),
        P(None, "dp", "tp"),
        P(None, "tp", None, None),
        P(None, "tp"),
        P(None, "tp", "dp"),
        P(None, ("grp", "dp"), "tp", None, None),
        P(None, ("grp", "dp"), "tp", None),
        P(None, ("grp", "dp"), "tp"),
    )
    out_specs = (
        P("grp", "dp"),
        P(None, ("grp", "dp"), "tp", None, None),
        P(None, ("grp", "dp"), "tp", None),
        P(None, ("grp", "dp"), "tp"),
    )
    return jax.shard_map(shards, mesh=mesh, in_specs=in_specs, out_specs=out_specs, check_vma=False)
```

profile of v0, /device:TPU:0, one launch (start us, length us, event | category | flops | bytes accessed | tf_op | source)
XLA Modules:
  0.0 279.2 jit_solution(203216173123310671)
XLA Ops:
  8.2 1.8 fusion.32
  10.1 1.8 fusion.30
  12.0 1.8 fusion.34
  13.8 1.8 fusion.28
  16.8 8.4 %psum.14 = f32[64]{0:T(128)S(1)} all-reduce(f32[64]{0:T(128)S(1)} %multiply_reduce_fusion.1), channel_id=1, replica_groups=mesh['grp'=2,'tp'=4,'dp'=4] {'dp'}, use_global_device_ids=true, to_apply=%region_1.0 | all-reduce | flops 64 | bytes 512 | tf_op jit(solution)/shard_map/psum | solution.py:42
  25.8 7.5 %reduce-scatter.13.cloned.1.call-done = f32[16,128]{1,0:T(8,128)} async-done(((f32[64,128]{1,0:T(8,128)}), f32[16,128]{1,0:T(8,128)}) %reduce-scatter.13.cloned.1.call-update) | async-done | bytes 8208 | tf_op jit(solution)/shard_map/reduce_scatter | solution.py:43
  33.3 22.0 %reduce-scatter.15.cloned.1.call-done = f32[16,128]{1,0:T(8,128)} async-done(((f32[64,128]{1,0:T(8,128)}), f32[16,128]{1,0:T(8,128)}) %reduce-scatter.15.cloned.1.call-update) | async-done | bytes 8208 | tf_op jit(solution)/shard_map/reduce_scatter | solution.py:43
  55.3 22.5 %reduce-scatter.11.cloned.1.call-done = f32[16,128]{1,0:T(8,128)} async-done(((f32[64,128]{1,0:T(8,128)}), f32[16,128]{1,0:T(8,128)}) %reduce-scatter.11.cloned.1.call-update) | async-done | bytes 8208 | tf_op jit(solution)/shard_map/reduce_scatter | solution.py:43
  81.1 18.6 %reduce-scatter.17.cloned.1.call-done = f32[16,128]{1,0:T(8,128)} async-done(((f32[64,128]{1,0:T(8,128)}), f32[16,128]{1,0:T(8,128)}) %reduce-scatter.17.cloned.1.call-update) | async-done | bytes 8208 | tf_op jit(solution)/shard_map/reduce_scatter | solution.py:43
  100.5 5.2 %all_gather.12 = bf16[64,128]{1,0:T(8,128)(2,1)S(1)} all-gather(bf16[16,128]{1,0:T(8,128)(2,1)S(1)} %multiply_convert_fusion.15), channel_id=1, replica_groups=mesh['grp'=2,'tp'=4,'dp'=4] {'dp'}, dimensions={0}, use_global_device_ids=true | all-gather | bytes 20480 | tf_op jit(solution)/shard_map/all_gather | solution.py:83
  106.7 20.1 %reduce-scatter.19.cloned.1.call-done = f32[16,1024]{1,0:T(8,128)} async-done(((f32[64,1024]{1,0:T(8,128)}), f32[16,1024]{1,0:T(8,128)}) %reduce-scatter.19.cloned.1.call-update) | async-done | bytes 65552 | tf_op jit(solution)/shard_map/reduce_scatter | solution.py:87
  127.6 13.4 %all_gather.13 = bf16[64,1024]{1,0:T(8,128)(2,1)S(1)} all-gather(bf16[16,1024]{1,0:T(8,128)(2,1)S(1)} %add_convert_fusion.1), channel_id=1, replica_groups=mesh['grp'=2,'tp'=4,'dp'=4] {'tp'}, dimensions={0}, use_global_device_ids=true | all-gather | bytes 163840 | tf_op jit(solution)/shard_map/all_gather | solution.py:91
  141.0 1.7 fusion.22
  142.7 1.7 fusion.20
  144.5 1.7 fusion.18
  146.3 1.7 fusion.24
  148.2 5.7 %psum.15 = f32[64]{0:T(128)S(1)} all-reduce(f32[64]{0:T(128)S(1)} %multiply_reduce_fusion), channel_id=1, replica_groups=mesh['grp'=2,'tp'=4,'dp'=4] {'dp'}, use_global_device_ids=true, to_apply=%region_9.10 | all-reduce | flops 64 | bytes 512 | tf_op jit(solution)/shard_map/psum | solution.py:42
  154.7 9.3 %reduce-scatter.23.cloned.1.call-done = f32[16,128]{1,0:T(8,128)} async-done(((f32[64,128]{1,0:T(8,128)}), f32[16,128]{1,0:T(8,128)}) %reduce-scatter.23.cloned.1.call-update) | async-done | bytes 8208 | tf_op jit(solution)/shard_map/reduce_scatter | solution.py:43
  164.0 22.0 %reduce-scatter.25.cloned.1.call-done = f32[16,128]{1,0:T(8,128)} async-done(((f32[64,128]{1,0:T(8,128)}), f32[16,128]{1,0:T(8,128)}) %reduce-scatter.25.cloned.1.call-update) | async-done | bytes 8208 | tf_op jit(solution)/shard_map/reduce_scatter | solution.py:43
  186.0 22.5 %reduce-scatter.21.cloned.1.call-done = f32[16,128]{1,0:T(8,128)} async-done(((f32[64,128]{1,0:T(8,128)}), f32[16,128]{1,0:T(8,128)}) %reduce-scatter.21.cloned.1.call-update) | async-done | bytes 8208 | tf_op jit(solution)/shard_map/reduce_scatter | solution.py:43
  213.1 17.4 %reduce-scatter.27.cloned.1.call-done = f32[16,128]{1,0:T(8,128)} async-done(((f32[64,128]{1,0:T(8,128)}), f32[16,128]{1,0:T(8,128)}) %reduce-scatter.27.cloned.1.call-update) | async-done | bytes 8208 | tf_op jit(solution)/shard_map/reduce_scatter | solution.py:43
  231.3 5.2 %all_gather.14 = bf16[64,128]{1,0:T(8,128)(2,1)S(1)} all-gather(bf16[16,128]{1,0:T(8,128)(2,1)S(1)} %multiply_convert_fusion.10), channel_id=1, replica_groups=mesh['grp'=2,'tp'=4,'dp'=4] {'dp'}, dimensions={0}, use_global_device_ids=true | all-gather | bytes 20480 | tf_op jit(solution)/shard_map/all_gather | solution.py:83
  240.8 16.8 %reduce-scatter.29.cloned.1.call-done = f32[16,1024]{1,0:T(8,128)} async-done(((f32[64,1024]{1,0:T(8,128)}), f32[16,1024]{1,0:T(8,128)}) %reduce-scatter.29.cloned.1.call-update) | async-done | bytes 65552 | tf_op jit(solution)/shard_map/reduce_scatter | solution.py:87
  258.4 13.4 %all_gather.15 = bf16[64,1024]{1,0:T(8,128)(2,1)S(1)} all-gather(bf16[16,1024]{1,0:T(8,128)(2,1)S(1)} %add_convert_fusion), channel_id=1, replica_groups=mesh['grp'=2,'tp'=4,'dp'=4] {'tp'}, dimensions={0}, use_global_device_ids=true | all-gather | bytes 163840 | tf_op jit(solution)/shard_map/all_gather | solution.py:91
  (72 shorter events, 20.9 us)
Async XLA Ops:
  7.2 18.0 %copy-start.5 = (f32[2,1]{0,1:T(1,128)S(1)}, f32[2,1]{0,1:T(1,128)}, u32[]{:S(2)}) copy-start(f32[2,1]{0,1:T(1,128)} %param.19) | copy-start | bytes 28
  7.2 71.5 %copy-start.6 = (bf16[2,1,384,2]{2,3,1,0:T(2,128)(2,1)S(1)}, bf16[2,1,384,2]{2,3,1,0:T(2,128)(2,1)}, u32[]{:S(2)}) copy-start(bf16[2,1,384,2]{2,3,1,0:T(2,128)(2,1)} %param.18) | copy-start | bytes 9220
  7.2 71.6 %copy-start.4 = (f32[2,16,1]{1,2,0:T(1,128)S(1)}, f32[2,16,1]{1,2,0:T(1,128)}, u32[]{:S(2)}) copy-start(f32[2,16,1]{1,2,0:T(1,128)} %param.23) | copy-start | bytes 388
  7.2 73.0 %copy-start.3 = (f32[2,16,1,128]{3,2,1,0:T(1,128)S(1)}, f32[2,16,1,128]{3,2,1,0:T(1,128)}, u32[]{:S(2)}) copy-start(f32[2,16,1,128]{3,2,1,0:T(1,128)} %param.22) | copy-start | bytes 49156
  7.2 73.1 %copy-start = (f32[2,16,1,128,128]{4,3,2,1,0:T(8,128)S(1)}, f32[2,16,1,128,128]{4,3,2,1,0:T(8,128)}, u32[]{:S(2)}) copy-start(f32[2,16,1,128,128]{4,3,2,1,0:T(8,128)} %param.21) | copy-start | bytes 6291460
  7.2 98.5 %copy-start.2 = (bf16[2,128,1024]{2,1,0:T(8,128)(2,1)S(1)}, bf16[2,128,1024]{2,1,0:T(8,128)(2,1)}, u32[]{:S(2)}) copy-start(bf16[2,128,1024]{2,1,0:T(8,128)(2,1)} %param.20) | copy-start | bytes 1572868
  7.2 26.1 %reduce-scatter.13.cloned.1.call-start = ((), (), s32[]{:S(2)}) async-start(), calls=%async_computation.11 | async-start | bytes 40960 | tf_op jit(solution)/shard_map/reduce_scatter | solution.py:43
  8.1 98.5 %copy-start.1 = (bf16[64,1024]{1,0:T(8,128)(2,1)S(1)}, bf16[64,1024]{1,0:T(8,128)(2,1)}, u32[]{:S(2)}) copy-start(bf16[64,1024]{1,0:T(8,128)(2,1)} %param.12) | copy-start | bytes 393220
  10.0 45.3 %reduce-scatter.15.cloned.1.call-start = ((), (), s32[]{:S(2)}) async-start(), calls=%async_computation.12 | async-start | bytes 40960 | tf_op jit(solution)/shard_map/reduce_scatter | solution.py:43
  11.9 65.9 %reduce-scatter.11.cloned.1.call-start = ((), (), s32[]{:S(2)}) async-start(), calls=%async_computation.10 | async-start | bytes 40960 | tf_op jit(solution)/shard_map/reduce_scatter | solution.py:43
  13.8 85.9 %reduce-scatter.17.cloned.1.call-start = ((), (), s32[]{:S(2)}) async-start(), calls=%async_computation.13 | async-start | bytes 40960 | tf_op jit(solution)/shard_map/reduce_scatter | solution.py:43
  15.7 111.1 %reduce-scatter.19.cloned.1.call-start = ((), (), s32[]{:S(2)}) async-start(), calls=%async_computation.14 | async-start | bytes 327680 | tf_op jit(solution)/shard_map/reduce_scatter | solution.py:87
  106.6 57.5 %reduce-scatter.23.cloned.1.call-start = ((), (), s32[]{:S(2)}) async-start(), calls=%async_computation.16 | async-start | bytes 40960 | tf_op jit(solution)/shard_map/reduce_scatter | solution.py:43
  146.2 39.8 %reduce-scatter.25.cloned.1.call-start = ((), (), s32[]{:S(2)}) async-start(), calls=%async_computation.17 | async-start | bytes 40960 | tf_op jit(solution)/shard_map/reduce_scatter | solution.py:43
  148.1 60.5 %reduce-scatter.21.cloned.1.call-start = ((), (), s32[]{:S(2)}) async-start(), calls=%async_computation.15 | async-start | bytes 40960 | tf_op jit(solution)/shard_map/reduce_scatter | solution.py:43
  153.9 76.6 %reduce-scatter.27.cloned.1.call-start = ((), (), s32[]{:S(2)}) async-start(), calls=%async_computation.18 | async-start | bytes 40960 | tf_op jit(solution)/shard_map/reduce_scatter | solution.py:43
  154.7 102.9 %reduce-scatter.29.cloned.1.call-start = ((), (), s32[]{:S(2)}) async-start(), calls=%async_computation.19 | async-start | bytes 327680 | tf_op jit(solution)/shard_map/reduce_scatter | solution.py:87
Sparse Core Ops, SparseCore 0:
  11.0 22.2 reduce-scatter.12
  35.7 19.5 reduce-scatter.14
  58.3 19.5 reduce-scatter.10
  80.1 19.5 reduce-scatter.16
  106.7 19.9 reduce-scatter.18
  146.3 17.6 reduce-scatter.22
  166.5 19.5 reduce-scatter.24
  189.0 19.5 reduce-scatter.20
  210.9 19.5 reduce-scatter.26
  237.5 19.9 reduce-scatter.28
where the time goes:
time: 280 us; the launch traced here: 279 us
  waiting for transfers between devices  179 us (64%)
  blocking collectives  51.2 us (18%)
  matrix products  17.7 us (6%)
  between operations  14.3 us (5%)
  other arithmetic  14 us (5%)
    reduce_scatter x8, waiting for transfers between devices, shards(): summed = lax.psum_scatter(terms, 'dp', scatter_dimension=0, tiled=True)  142 us
    reduce_scatter x2, waiting for transfers between devices, shards(): mine = lax.psum_scatter(partial_mix, 'tp', scatter_dimension=0, tiled=True)  36.9 us
    all_gather x2, blocking collectives, shards(): x = lax.all_gather(updated, 'tp', axis=0, tiled=True)  26.7 us
    dot_general x8, matrix products, shards(): jnp.dot(scaled_in, weight[blk], preferred_element_type=jnp.float32)  14.2 us
    psum x2, blocking collectives, shards(): totals = lax.psum(squares, 'dp')  14 us
    all_gather x2, blocking collectives, shards(): lax.all_gather(gated, 'dp', axis=0, tiled=True)  10.4 us
  transfers between devices with their start and end apart: 10, of which 10 were waited for; matrix products, arithmetic and copies ran while one was open for 7% of the time, Pallas kernels for 0%

commit v1 on v0

v1 whole, which is shorter than its diff:
```python
import functools

import jax
import jax.numpy as jnp
from jax import lax
from jax.experimental import pallas as pl
from jax.experimental.pallas import tpu as pltpu
from jax.sharding import PartitionSpec as P

EPS = 1e-06
F32 = jnp.float32
BF16 = jnp.bfloat16
MESH = pl.DeviceIdType.MESH


def step_kernel(
    n, m, features,
    tokens, gain, w_query, w_key, w_value, w_outgate, gate_w, w_mix, memory, normalizer, stabilizer, bias,
    x_out, keep_out, value_out, key_out, norm_out, stab_out,
    gain_v, w_v, gate_v, mix_v, mem_v, norm_v, stab_v,
    x_v, xf_v, part_send, part_own, part_recv, gated_v, mix_f, mix_send, mix_own, mix_recv,
    load_sem, ps_sem, pr_sem, gs_sem, gr_sem, ms_sem, mr_sem, xs_sem, xr_sem,
):
    blocks = memory.shape[0]
    own, heads, dk = memory.shape[1], memory.shape[2], memory.shape[3]
    rows = x_v.shape[2]
    width = heads * dk
    dp, tp = lax.axis_index("dp"), lax.axis_index("tp")

    def load(k, src, dst):
        return pltpu.make_async_copy(src, dst, load_sem.at[k])

    loads = {}
    order = [("x", 0, tokens, x_v.at[0]), ("g", 0, gain, gain_v)]
    for b in range(blocks):
        for k, w in enumerate((w_query, w_key, w_value, w_outgate)):
            order.append((f"w{k}", b, w.at[b], w_v.at[b, :, pl.ds(k * width, width)]))
        if b == 0:
            order.append(("gate", 0, gate_w, gate_v))
            order.append(("norm", 0, normalizer, norm_v))
            order.append(("stab", 0, stabilizer, stab_v))
        order.append(("mem", b, memory.at[b], mem_v.at[b]))
        order.append(("mix", b, w_mix.at[b], mix_v.at[b]))
    for k, (name, b, src, dst) in enumerate(order):
        loads[name, b] = load(k, src, dst)
        loads[name, b].start()

    barrier = pltpu.get_barrier_semaphore()
    for o in range(1, n):
        pl.semaphore_signal(barrier, inc=1, device_id={"dp": lax.rem(dp + o, n)}, device_id_type=MESH)
    for o in range(1, m):
        pl.semaphore_signal(barrier, inc=1, device_id={"tp": lax.rem(tp + o, m)}, device_id_type=MESH)

    def send(src, dst, s_sem, r_sem, axis, size, me, o):
        return pltpu.make_async_remote_copy(
            src_ref=src, dst_ref=dst, send_sem=s_sem, recv_sem=r_sem,
            device_id={axis: lax.rem(me + o, size)}, device_id_type=MESH,
        )

    sent = []
    loads["x", 0].wait()
    loads["g", 0].wait()
    for b in range(blocks):
        for j in range(m):
            xf_v[j * rows:(j + 1) * rows, :] = x_v[b, j].astype(F32)
        xf = xf_v[...]
        squares = jnp.sum(xf * xf, axis=-1, keepdims=True)
        scaled_in = (xf * gain_v[b:b + 1, :]).astype(BF16)
        for k in range(4):
            loads[f"w{k}", b].wait()
        part = jnp.dot(scaled_in, w_v[b], preferred_element_type=F32)
        lane = lax.broadcasted_iota(jnp.int32, (own, 128), 1)
        for j in range(n):
            piece = part[j * own:(j + 1) * own, :]
            sq = jnp.broadcast_to(squares[j * own:(j + 1) * own, :], (own, 128))
            high = sq.astype(BF16)
            low = (sq - high.astype(F32)).astype(BF16)
            part_send[b, j, :, : 4 * width] = piece.astype(BF16)
            part_send[b, j, :, 4 * width:] = jnp.where(lane < 64, high.astype(F32), low.astype(F32)).astype(BF16)
            part_own[j, :, : 4 * width] = piece
            part_own[j, :, 4 * width:] = jnp.where(lane < 64, sq, 0.0)
        if b == 0:
            pl.semaphore_wait(barrier, n - 1 + m - 1)
        copies = []
        for o in range(1, n):
            to = lax.rem(dp + o, n)
            c = send(part_send.at[b, to], part_recv.at[b, o - 1], ps_sem.at[b, o - 1], pr_sem.at[b, o - 1], "dp", n, dp, o)
            c.start()
            copies.append(c)
        total = part_own[dp]
        for o, c in enumerate(copies):
            c.wait_recv()
            total = total + part_recv[b, o].astype(F32)
        sent += copies
        own_sq = total[:, 4 * width:4 * width + 1] + total[:, 4 * width + 64:4 * width + 65]
        scale = lax.rsqrt(own_sq / features + EPS)
        projs = (scale * total[:, : 4 * width]).astype(BF16)
        if b == 0:
            loads["gate", 0].wait()
            loads["norm", 0].wait()
            loads["stab", 0].wait()
        loads["mem", b].wait()
        for h in range(heads):
            q16, k16, v16, o16 = (projs[:, k * width + h * dk:k * width + (h + 1) * dk] for k in range(4))
            query, key, value, outgate = (t.astype(F32) for t in (q16, k16, v16, o16))
            pre = (
                jnp.dot(q16, gate_v[b, h, :dk], preferred_element_type=F32)
                + jnp.dot(k16, gate_v[b, h, dk:2 * dk], preferred_element_type=F32)
                + jnp.dot(v16, gate_v[b, h, 2 * dk:], preferred_element_type=F32)
            )
            log_input = pre[:, 0:1]
            z = pre[:, 1:2] + bias[b, h]
            log_forget = jnp.minimum(z, 0.0) - jnp.log1p(jnp.exp(-jnp.abs(z)))
            stab = stab_v[b, :, h:h + 1]
            new_stab = jnp.maximum(log_forget + stab, log_input)
            keep = jnp.exp(log_forget + stab - new_stab)
            admit = jnp.exp(log_input - new_stab)
            ak = admit * (key * dk ** (-0.5))
            new_norm = keep * norm_v[b, :, h, :] + ak
            query_t = query.T
            held = jnp.concatenate(
                [jnp.sum(query_t[:, s:s + 1] * mem_v[b, s, h], axis=0, keepdims=True) for s in range(own)], axis=0
            )
            numer = keep * held + jnp.sum(query * ak, axis=-1, keepdims=True) * value
            denom = jnp.maximum(jnp.abs(jnp.sum(query * new_norm, axis=-1, keepdims=True)), 1.0)
            gated_v[b, dp, :, h * dk:(h + 1) * dk] = (numer / denom * jax.nn.sigmoid(outgate)).astype(BF16)
            stab_out[b, :, h:h + 1] = new_stab
            norm_out[b, :, h, :] = new_norm
            keep_out[b, h] = jnp.broadcast_to(keep, (own, dk))
            value_out[b, h] = value
            key_out[b, h] = ak.T
        copies = []
        for o in range(1, n):
            c = send(gated_v.at[b, dp], gated_v.at[b, dp], gs_sem.at[b, o - 1], gr_sem.at[b, o - 1], "dp", n, dp, o)
            c.start()
            copies.append(c)
        loads["mix", b].wait()
        for c in copies:
            c.wait_recv()
        sent += copies
        every = gated_v[b].reshape(n * own, width)
        mix_f[...] = jnp.dot(every, mix_v[b], preferred_element_type=F32)
        for j in range(m):
            piece = mix_f[j * rows:(j + 1) * rows, :]
            mix_send[b, j] = piece.astype(BF16)
            mix_own[j] = piece
        copies = []
        for o in range(1, m):
            to = lax.rem(tp + o, m)
            c = send(mix_send.at[b, to], mix_recv.at[b, o - 1], ms_sem.at[b, o - 1], mr_sem.at[b, o - 1], "tp", m, tp, o)
            c.start()
            copies.append(c)
        total = mix_own[tp]
        for o, c in enumerate(copies):
            c.wait_recv()
            total = total + mix_recv[b, o].astype(F32)
        sent += copies
        x_v[b + 1, tp] = (x_v[b, tp].astype(F32) + total).astype(BF16)
        copies = []
        for o in range(1, m):
            c = send(x_v.at[b + 1, tp], x_v.at[b + 1, tp], xs_sem.at[b, o - 1], xr_sem.at[b, o - 1], "tp", m, tp, o)
            c.start()
            copies.append(c)
        for c in copies:
            c.wait_recv()
        sent += copies
    x_out[...] = x_v[blocks]
    for c in sent:
        c.wait_send()


def state_kernel(memory, keep, value, key, x, norm, stab, new_memory, x_out, norm_out, stab_out):
    own, heads = memory.shape[1], memory.shape[2]
    for h in range(heads):
        keys = key[0, h]
        for s in range(own):
            new_memory[0, s, h] = (
                keep[0, h, s:s + 1, :] * memory[0, s, h] + keys[:, s:s + 1] * value[0, h, s:s + 1, :]
            )
    x_out[...] = x[...]
    norm_out[...] = norm[...]
    stab_out[...] = stab[...]


def shards(n, m, tokens, norm_gain, w_query, w_key, w_value, w_outgate, gate_weight, forget_bias, w_mix, memory, normalizer, stabilizer):
    seqs, feats = tokens.shape
    blocks, own, heads, dk, _ = memory.shape
    width = heads * dk
    rows = seqs // m
    cols = 4 * width + 128
    anywhere = pl.BlockSpec(memory_space=pl.ANY)
    vmem = pl.BlockSpec(memory_space=pltpu.VMEM)
    dma = pltpu.SemaphoreType.DMA
    nd, nt = max(n - 1, 1), max(m - 1, 1)
    sds = jax.ShapeDtypeStruct
    x, keep, value, key, norm, stab = pl.pallas_call(
        functools.partial(step_kernel, n, m, n * feats),
        out_shape=(
            sds((m, rows, feats), BF16),
            sds((blocks, heads, own, dk), F32),
            sds((blocks, heads, own, dk), F32),
            sds((blocks, heads, dk, own), F32),
            sds((blocks, own, heads, dk), F32),
            sds((blocks, own, heads), F32),
        ),
        in_specs=[anywhere] * 11 + [pl.BlockSpec(memory_space=pltpu.SMEM)],
        out_specs=(vmem,) * 6,
        scratch_shapes=[
            pltpu.VMEM(norm_gain.shape, F32),
            pltpu.VMEM((blocks, feats, 4 * width), BF16),
            pltpu.VMEM(gate_weight.shape, BF16),
            pltpu.VMEM(w_mix.shape, BF16),
            pltpu.VMEM(memory.shape, F32),
            pltpu.VMEM(normalizer.shape, F32),
            pltpu.VMEM(stabilizer.shape, F32),
            pltpu.VMEM((blocks + 1, m, rows, feats), BF16),
            pltpu.VMEM((seqs, feats), F32),
            pltpu.VMEM((blocks, n, own, cols), BF16),
            pltpu.VMEM((n, own, cols), F32),
            pltpu.VMEM((blocks, nd, own, cols), BF16),
            pltpu.VMEM((blocks, n, own, width), BF16),
            pltpu.VMEM((seqs, feats), F32),
            pltpu.VMEM((blocks, m, rows, feats), BF16),
            pltpu.VMEM((m, rows, feats), F32),
            pltpu.VMEM((blocks, nt, rows, feats), BF16),
            dma((5 + 6 * blocks,)),
            dma((blocks, nd)), dma((blocks, nd)), dma((blocks, nd)), dma((blocks, nd)),
            dma((blocks, nt)), dma((blocks, nt)), dma((blocks, nt)), dma((blocks, nt)),
        ],
        compiler_params=pltpu.CompilerParams(collective_id=0, has_side_effects=True),
    )(
        tokens.reshape(m, rows, feats), norm_gain, w_query, w_key, w_value, w_outgate,
        gate_weight, w_mix, memory, normalizer, stabilizer, forget_bias,
    )

    def per_block(shape):
        return pl.BlockSpec((1,) + shape[1:], lambda b: (b,) + (0,) * (len(shape) - 1))

    def whole(shape):
        return pl.BlockSpec(shape, lambda b: (0,) * len(shape))

    new_memory, x, norm, stab = pl.pallas_call(
        state_kernel,
        grid=(blocks,),
        out_shape=(sds(memory.shape, F32), sds(x.shape, BF16), sds(norm.shape, F32), sds(stab.shape, F32)),
        in_specs=[per_block(t.shape) for t in (memory, keep, value, key)] + [whole(t.shape) for t in (x, norm, stab)],
        out_specs=(per_block(memory.shape), whole(x.shape), whole(norm.shape), whole(stab.shape)),
    )(memory, keep, value, key, x, norm, stab)
    return x.reshape(seqs, feats), new_memory, norm, stab


def solution(mesh):
    in_specs = (
        P("grp", "dp"),
        P(None, "dp"),
        P(None, "dp", "tp"),
        P(None, "dp", "tp"),
        P(None, "dp", "tp"),
        P(None, "dp", "tp"),
        P(None, "tp", None, None),
        P(None, "tp"),
        P(None, "tp", "dp"),
        P(None, ("grp", "dp"), "tp", None, None),
        P(None, ("grp", "dp"), "tp", None),
        P(None, ("grp", "dp"), "tp"),
    )
    out_specs = (
        P("grp", "dp"),
        P(None, ("grp", "dp"), "tp", None, None),
        P(None, ("grp", "dp"), "tp", None),
        P(None, ("grp", "dp"), "tp"),
    )
    body = functools.partial(shards, mesh.shape["dp"], mesh.shape["tp"])
    return jax.shard_map(body, mesh=mesh, in_specs=in_specs, out_specs=out_specs, check_vma=False)
```

time: 280 us -> 47.4 us (0.17)
  waiting for transfers between devices: 179 us -> 0 us
  blocking collectives: 51.2 us -> 0 us
  Pallas kernels: 0 us -> 40.9 us
  matrix products: 17.7 us -> 0 us
  other arithmetic: 14 us -> 0 us
  between operations: 14.3 us -> 0.64 us
  local copies, waits for them, and re-layouts: 2.14 us -> 5.54 us
    reduce_scatter x10 -> x0, waiting for transfers between devices: 179 us -> none  [the longest x8 142 us: shards(): summed = lax.psum_scatter(terms, 'dp', scatter_dimension=0, tiled=True)]
    pallas_call x0 -> x2, Pallas kernels: none -> 40.9 us  [the longest x1 37.9 us: shards(): pl.pallas_call(functools.partial(step_kernel, n, m, n * feats), out_shape...]
    all_gather x4 -> x0, blocking collectives: 37.2 us -> none  [the longest x2 26.7 us: shards(): x = lax.all_gather(updated, 'tp', axis=0, tiled=True)]
    dot_general x14 -> x0, matrix products: 17.7 us -> none  [the longest x8 14.2 us: shards(): jnp.dot(scaled_in, weight[blk], preferred_element_type=jnp.float32)]
    psum x2 -> x0, blocking collectives: 14 us -> none  [shards(): totals = lax.psum(squares, 'dp')]
    unnamed x15 -> x4, local copies, waits for them, and re-layouts: 0.69 us -> 5.54 us
    convert_element_type x6 -> x0, other arithmetic: 3.29 us -> none  [the longest x2 1.7 us: shards(): updated = (own_rows + mine).astype(jnp.bfloat16)]
    another operation x5 -> x0, other arithmetic: 3.01 us -> none  [the longest x1 1.46 us: shards(): jnp.stack(mems, axis=0)]
  transfers between devices with their start and end apart: 10 -> 0, of which waited for: 10 -> 0; matrix products, arithmetic and copies ran while one was open for 7% -> 0% of each run, Pallas kernels for 0% -> 0%
where the time goes in v1:
time: 47.4 us; the launch traced here: 47.1 us
  Pallas kernels  40.9 us (86%)
  local copies, waits for them, and re-layouts  5.54 us (12%)
  between operations  0.64 us (1%)
    pallas_call x1, Pallas kernels, shards(): pl.pallas_call(functools.partial(step_kernel, n, m, n * feats), out_shape...  37.9 us
    unnamed x4, local copies, waits for them, and re-layouts  5.54 us
    pallas_call x1, Pallas kernels, shards(): pl.pallas_call(state_kernel, grid=(blocks,), out_shape=(sds(memory.shape,...  3.07 us

profile of v1, /device:TPU:0, one launch (start us, length us, event | category | flops | bytes accessed | tf_op | source)
XLA Modules:
  0.0 47.1 jit_solution(10709443056495887325)
XLA Ops:
  0.6 1.3 %copy.18.bias = f32[2,1]{1,0:T(2,128)} copy(f32[2,1]{0,1:T(1,128)} %param.19) | data formatting | bytes 16 | tf_op args[7]
  1.9 1.4 %copy.17.stabilizer = f32[2,16,1]{2,1,0:T(8,128)} copy(f32[2,16,1]{1,2,0:T(1,128)} %param.23) | data formatting | bytes 256 | tf_op args[11]
  3.3 1.5 %copy.16.gate_w = bf16[2,1,384,2]{3,2,1,0:T(8,128)(2,1)} copy(bf16[2,1,384,2]{2,3,1,0:T(2,128)(2,1)} %param.18) | data formatting | bytes 6144 | tf_op args[6]
  4.8 37.9 %shard_map.147 = (bf16[4,16,1024]{2,1,0:T(8,128)(2,1)}, f32[2,1,16,128]{3,2,1,0:T(8,128)}, f32[2,1,16,128]{3,2,1,0:T(8,128)}, f32[2,1,128,16]{3,2,1,0:T(8,128)},...) custom-call(bf16[4,16,1024]{2,1,0:T(8,128)(2,1)} %bitcast.2, f32[2,1024]{1,0:T(2,128)} %gain.1, ...), custom_call_target="tpu_custom_call" | custom-call | tf_op jit(solution)/shard_map/pallas_call | solution.py:196
  42.7 3.1 %shard_map.148 = (f32[2,16,1,128,128]{4,3,2,1,0:T(8,128)}, bf16[4,16,1024]{2,1,0:T(8,128)(2,1)}, f32[2,16,1,128]{3,2,1,0:T(1,128)}, f32[2,16,1]{2,1,0:T(8,128)}) custom-call(f32[2,16,1,128,128]{4,3,2,1,0:T(8,128)} %memory.3, f32[2,1,16,128]{3,2,1,0:T(8,128)} %get-tuple-element.14.keep, f32[2,1,16,128]{3,2,1,0:T(8,128)} %get-tuple-element.15.value, ...), custom_call_target="tpu_custom_call" | custom-call | tf_op jit(solution)/shard_map/pallas_call | solution.py:242
  45.7 1.4 %copy.19 = f32[2,16,1]{1,2,0:T(1,128)} copy(f32[2,16,1]{2,1,0:T(8,128)} %get-tuple-element.27) | data formatting | bytes 256

commit v2 on v1

--- a/solution.py
+++ b/solution.py
@@ -58,6 +58,7 @@
         )
 
     sent = []
+    diagonal = lax.broadcasted_iota(jnp.int32, (own, own), 0) == lax.broadcasted_iota(jnp.int32, (own, own), 1)
     loads["x", 0].wait()
     loads["g", 0].wait()
     for b in range(blocks):
@@ -101,22 +102,26 @@
             loads["stab", 0].wait()
         loads["mem", b].wait()
         for h in range(heads):
-            q16, k16, v16, o16 = (projs[:, k * width + h * dk:k * width + (h + 1) * dk] for k in range(4))
-            query, key, value, outgate = (t.astype(F32) for t in (q16, k16, v16, o16))
-            pre = (
-                jnp.dot(q16, gate_v[b, h, :dk], preferred_element_type=F32)
-                + jnp.dot(k16, gate_v[b, h, dk:2 * dk], preferred_element_type=F32)
-                + jnp.dot(v16, gate_v[b, h, 2 * dk:], preferred_element_type=F32)
+            query, key, value, outgate = (
+                projs[:, k * width + h * dk:k * width + (h + 1) * dk].astype(F32) for k in range(4)
             )
-            log_input = pre[:, 0:1]
-            z = pre[:, 1:2] + bias[b, h]
+            gate = gate_v[b, h].astype(F32)
+
+            def pre(g):
+                terms = (
+                    query * gate[g:g + 1, :dk] + key * gate[g:g + 1, dk:2 * dk] + value * gate[g:g + 1, 2 * dk:]
+                )
+                return jnp.sum(terms, axis=-1, keepdims=True)
+
+            log_input = pre(0)
+            z = pre(1) + bias[h, b]
             log_forget = jnp.minimum(z, 0.0) - jnp.log1p(jnp.exp(-jnp.abs(z)))
-            stab = stab_v[b, :, h:h + 1]
+            stab = jnp.sum(jnp.where(diagonal, stab_v[b, h:h + 1, :], 0.0), axis=1, keepdims=True)
             new_stab = jnp.maximum(log_forget + stab, log_input)
             keep = jnp.exp(log_forget + stab - new_stab)
             admit = jnp.exp(log_input - new_stab)
             ak = admit * (key * dk ** (-0.5))
-            new_norm = keep * norm_v[b, :, h, :] + ak
+            new_norm = keep * norm_v[b, :, h * dk:(h + 1) * dk] + ak
             query_t = query.T
             held = jnp.concatenate(
                 [jnp.sum(query_t[:, s:s + 1] * mem_v[b, s, h], axis=0, keepdims=True) for s in range(own)], axis=0
@@ -124,8 +129,8 @@
             numer = keep * held + jnp.sum(query * ak, axis=-1, keepdims=True) * value
             denom = jnp.maximum(jnp.abs(jnp.sum(query * new_norm, axis=-1, keepdims=True)), 1.0)
             gated_v[b, dp, :, h * dk:(h + 1) * dk] = (numer / denom * jax.nn.sigmoid(outgate)).astype(BF16)
-            stab_out[b, :, h:h + 1] = new_stab
-            norm_out[b, :, h, :] = new_norm
+            stab_out[b, h:h + 1, :] = jnp.sum(jnp.where(diagonal, new_stab, 0.0), axis=0, keepdims=True)
+            norm_out[b, :, h * dk:(h + 1) * dk] = new_norm
             keep_out[b, h] = jnp.broadcast_to(keep, (own, dk))
             value_out[b, h] = value
             key_out[b, h] = ak.T
@@ -200,19 +205,19 @@
             sds((blocks, heads, own, dk), F32),
             sds((blocks, heads, own, dk), F32),
             sds((blocks, heads, dk, own), F32),
-            sds((blocks, own, heads, dk), F32),
-            sds((blocks, own, heads), F32),
+            sds((blocks, own, width), F32),
+            sds((blocks, heads, own), F32),
         ),
         in_specs=[anywhere] * 11 + [pl.BlockSpec(memory_space=pltpu.SMEM)],
         out_specs=(vmem,) * 6,
         scratch_shapes=[
             pltpu.VMEM(norm_gain.shape, F32),
             pltpu.VMEM((blocks, feats, 4 * width), BF16),
-            pltpu.VMEM(gate_weight.shape, BF16),
+            pltpu.VMEM((blocks, heads, 2, 3 * dk), BF16),
             pltpu.VMEM(w_mix.shape, BF16),
             pltpu.VMEM(memory.shape, F32),
-            pltpu.VMEM(normalizer.shape, F32),
-            pltpu.VMEM(stabilizer.shape, F32),
+            pltpu.VMEM((blocks, own, width), F32),
+            pltpu.VMEM((blocks, heads, own), F32),
             pltpu.VMEM((blocks + 1, m, rows, feats), BF16),
             pltpu.VMEM((seqs, feats), F32),
             pltpu.VMEM((blocks, n, own, cols), BF16),
@@ -230,7 +235,8 @@
         compiler_params=pltpu.CompilerParams(collective_id=0, has_side_effects=True),
     )(
         tokens.reshape(m, rows, feats), norm_gain, w_query, w_key, w_value, w_outgate,
-        gate_weight, w_mix, memory, normalizer, stabilizer, forget_bias,
+        jnp.swapaxes(gate_weight, 2, 3), w_mix, memory, normalizer.reshape(blocks, own, width),
+        jnp.swapaxes(stabilizer, 1, 2), forget_bias.T,
     )
 
     def per_block(shape):
@@ -246,7 +252,7 @@
         in_specs=[per_block(t.shape) for t in (memory, keep, value, key)] + [whole(t.shape) for t in (x, norm, stab)],
         out_specs=(per_block(memory.shape), whole(x.shape), whole(norm.shape), whole(stab.shape)),
     )(memory, keep, value, key, x, norm, stab)
-    return x.reshape(seqs, feats), new_memory, norm, stab
+    return x.reshape(seqs, feats), new_memory, norm.reshape(normalizer.shape), jnp.swapaxes(stab, 1, 2)
 
 
 def solution(mesh):

time: 47.4 us -> 41.5 us (0.88)
  local copies, waits for them, and re-layouts: 5.54 us -> 0 us
    unnamed x4 -> x0, local copies, waits for them, and re-layouts: 5.54 us -> none
where the time goes in v2:
time: 41.5 us; the launch traced here: 41.4 us
  Pallas kernels  40.7 us (98%)
  between operations  0.64 us (2%)
    pallas_call x1, Pallas kernels, shards(): pl.pallas_call(functools.partial(step_kernel, n, m, n * feats), out_shape...  37.6 us
    pallas_call x1, Pallas kernels, shards(): pl.pallas_call(state_kernel, grid=(blocks,), out_shape=(sds(memory.shape,...  3.07 us

profile of v2, /device:TPU:0, one launch (start us, length us, event | category | flops | bytes accessed | tf_op | source)
XLA Modules:
  0.0 41.4 jit_solution(3937060022910074116)
XLA Ops:
  0.6 37.6 %shard_map.147 = (bf16[4,16,1024]{2,1,0:T(8,128)(2,1)}, f32[2,1,16,128]{3,2,1,0:T(8,128)}, f32[2,1,16,128]{3,2,1,0:T(8,128)}, f32[2,1,128,16]{3,2,1,0:T(8,128)},...) custom-call(bf16[4,16,1024]{2,1,0:T(8,128)(2,1)} %bitcast.14, f32[2,1024]{1,0:T(2,128)} %gain.1, ...), custom_call_target="tpu_custom_call" | custom-call | tf_op jit(solution)/shard_map/pallas_call | solution.py:201
  38.3 3.1 %shard_map.148 = (f32[2,16,1,128,128]{4,3,2,1,0:T(8,128)}, bf16[4,16,1024]{2,1,0:T(8,128)(2,1)}, f32[2,16,128]{2,1,0:T(8,128)}, f32[2,1,16]{2,1,0:T(1,128)}) custom-call(f32[2,16,1,128,128]{4,3,2,1,0:T(8,128)} %memory.3, f32[2,1,16,128]{3,2,1,0:T(8,128)} %get-tuple-element.14.keep, f32[2,1,16,128]{3,2,1,0:T(8,128)} %get-tuple-element.15.value, ...), custom_call_target="tpu_custom_call" | custom-call | tf_op jit(solution)/shard_map/pallas_call | solution.py:248

commit v3 on v2

v3 whole, which is shorter than its diff:
```python
import functools

import jax
import jax.numpy as jnp
from jax import lax
from jax.experimental import pallas as pl
from jax.experimental.pallas import tpu as pltpu
from jax.sharding import PartitionSpec as P

EPS = 1e-06
F32 = jnp.float32
BF16 = jnp.bfloat16
MESH = pl.DeviceIdType.MESH


def step_kernel(
    sizes, fast,
    tokens, gain, w_query, w_key, w_value, w_outgate, gate_w, w_mix, memory, normalizer, stabilizer, bias,
    x_out, memory_out, norm_out, stab_out,
    gain_v, w_v, gate_v, mix_v, mixcol_v, mem_v, norm_v, stab_v, tokens_v, xf_v, part_send, part_own, part_recv,
    gated_v, xcol_v, mix_send, mix_own, mix_recv, xrow_v,
    load_sem, ps_sem, pr_sem, gs_sem, gr_sem, ms_sem, mr_sem, xs_sem, xr_sem, zs_sem, zr_sem, ys_sem, yr_sem,
):
    groups, n, m = sizes
    blocks = memory.shape[0]
    own, heads, dk = memory.shape[1], memory.shape[2], memory.shape[3]
    seqs, feats = tokens.shape
    features = n * feats
    rows, cols = seqs // m, feats // m
    width = heads * dk
    share = width // groups
    grp, dp, tp = lax.axis_index("grp"), lax.axis_index("dp"), lax.axis_index("tp")
    last = blocks - 1

    def mix_slot(b, t):
        return mix_v.at[t] if b == last else mixcol_v.at[b, t]

    def mix_cols(b, to):
        return pl.ds(0, feats) if b == last else pl.ds(pl.multiple_of(to * cols, cols), cols)

    order = [("x", 0, tokens, tokens_v), ("g", 0, gain, gain_v)]
    for b in range(blocks):
        for k, w in enumerate((w_query, w_key, w_value, w_outgate)):
            order.append((f"w{k}", b, w.at[b], w_v.at[b, :, pl.ds(k * width, width)]))
        if b == 0:
            order.append(("gate", 0, gate_w, gate_v))
            order.append(("norm", 0, normalizer, norm_v))
            order.append(("stab", 0, stabilizer, stab_v))
        order.append(("mem", b, memory.at[b], mem_v.at[b]))
        if fast:
            order.append(("mix", b, w_mix.at[b, :, mix_cols(b, tp)], mix_slot(b, tp)))
        else:
            order.append(("mix", b, w_mix.at[b], mix_v.at[b]))
    loads = {}
    for k, (name, b, src, dst) in enumerate(order):
        loads[name, b] = pltpu.make_async_copy(src, dst, load_sem.at[k])
        loads[name, b].start()

    if fast:
        peers = [(od, ot) for ot in range(m) for od in range(n) if (od, ot) != (0, 0)]
    else:
        peers = [(od, 0) for od in range(1, n)] + [(0, ot) for ot in range(1, m)]
    barrier = pltpu.get_barrier_semaphore()

    def at(od, ot, og=0):
        return {"grp": lax.rem(grp + og, groups), "dp": lax.rem(dp + od, n), "tp": lax.rem(tp + ot, m)}

    for od, ot in peers:
        pl.semaphore_signal(barrier, inc=1, device_id=at(od, ot), device_id_type=MESH)
    greeted = len(peers)
    if fast:
        for og in range(1, groups):
            pl.semaphore_signal(barrier, inc=1, device_id=at(0, 0, og), device_id_type=MESH)
        greeted += groups - 1

    sent = []

    def send(src, dst, s_sem, r_sem, where):
        c = pltpu.make_async_remote_copy(
            src_ref=src, dst_ref=dst, send_sem=s_sem, recv_sem=r_sem, device_id=where, device_id_type=MESH
        )
        c.start()
        sent.append(c)
        return c

    def spread(b, offsets):
        part = pl.ds(pl.multiple_of(grp * share, share), share)
        return [
            (o, send(w_mix.at[b, part, mix_cols(b, lax.rem(tp + o, m))], mix_slot(b, tp).at[part],
                     zs_sem.at[b, o - 1], zr_sem.at[b, o - 1], at(0, o)))
            for o in offsets
        ]

    def relay(b, arriving):
        part = pl.ds(pl.multiple_of(grp * share, share), share)
        out = []
        for o, c in arriving:
            c.wait_recv()
            ref = mix_slot(b, lax.rem(tp + m - o, m)).at[part]
            for og in range(1, groups):
                out.append(send(ref, ref, ys_sem.at[b, o - 1, og - 1], yr_sem.at[b, o - 1, og - 1], at(0, 0, og)))
        return out

    diagonal = lax.broadcasted_iota(jnp.int32, (own, own), 0) == lax.broadcasted_iota(jnp.int32, (own, own), 1)
    lane = lax.broadcasted_iota(jnp.int32, (own, 128), 1)
    pending, relayed = {b: [] for b in range(blocks)}, {b: [] for b in range(blocks)}
    loads["x", 0].wait()
    loads["g", 0].wait()
    xf_v[...] = tokens_v[...].astype(F32)
    for b in range(blocks):
        xf = xf_v[...]
        squares = jnp.sum(xf * xf, axis=-1, keepdims=True)
        scaled_in = (xf * gain_v[b:b + 1, :]).astype(BF16)
        if b == 0:
            pl.semaphore_wait(barrier, greeted)
            if fast:
                pending[0] = spread(0, range(1, m))
        for k in range(4):
            loads[f"w{k}", b].wait()
        part = jnp.dot(scaled_in, w_v[b], preferred_element_type=F32)
        for j in range(n):
            piece = part[j * own:(j + 1) * own, :]
            sq = jnp.broadcast_to(squares[j * own:(j + 1) * own, :], (own, 128))
            high = sq.astype(BF16)
            low = (sq - high.astype(F32)).astype(BF16)
            part_send[b, j, :, : 4 * width] = piece.astype(BF16)
            part_send[b, j, :, 4 * width:] = jnp.where(lane < 64, high.astype(F32), low.astype(F32)).astype(BF16)
            part_own[j, :, : 4 * width] = piece
            part_own[j, :, 4 * width:] = jnp.where(lane < 64, sq, 0.0)
        copies = [
            send(part_send.at[b, lax.rem(dp + o, n)], part_recv.at[b, o - 1],
                 ps_sem.at[b, o - 1], pr_sem.at[b, o - 1], at(o, 0))
            for o in range(1, n)
        ]
        if b == 0:
            loads["gate", 0].wait()
            loads["norm", 0].wait()
            loads["stab", 0].wait()
        loads["mem", b].wait()
        total = part_own[dp]
        for o, c in enumerate(copies):
            c.wait_recv()
            total = total + part_recv[b, o].astype(F32)
        own_sq = total[:, 4 * width:4 * width + 1] + total[:, 4 * width + 64:4 * width + 65]
        scale = lax.rsqrt(own_sq / features + EPS)
        projs = (scale * total[:, : 4 * width]).astype(BF16)
        mine = gated_v.at[b, tp if fast else 0, dp]
        updates = []
        for h in range(heads):
            query, key, value, outgate = (
                projs[:, k * width + h * dk:k * width + (h + 1) * dk].astype(F32) for k in range(4)
            )
            gate = gate_v[b, h].astype(F32)

            def pre(g):
                terms = (
                    query * gate[g:g + 1, :dk] + key * gate[g:g + 1, dk:2 * dk] + value * gate[g:g + 1, 2 * dk:]
                )
                return jnp.sum(terms, axis=-1, keepdims=True)

            log_input = pre(0)
            z = pre(1) + bias[h, b]
            log_forget = jnp.minimum(z, 0.0) - jnp.log1p(jnp.exp(-jnp.abs(z)))
            stab = jnp.sum(jnp.where(diagonal, stab_v[b, h:h + 1, :], 0.0), axis=1, keepdims=True)
            new_stab = jnp.maximum(log_forget + stab, log_input)
            keep = jnp.exp(log_forget + stab - new_stab)
            admit = jnp.exp(log_input - new_stab)
            ak = admit * (key * dk ** (-0.5))
            new_norm = keep * norm_v[b, :, h * dk:(h + 1) * dk] + ak
            query_t = query.T
            held = jnp.concatenate(
                [jnp.sum(query_t[:, s:s + 1] * mem_v[b, s, h], axis=0, keepdims=True) for s in range(own)], axis=0
            )
            numer = keep * held + jnp.sum(query * ak, axis=-1, keepdims=True) * value
            denom = jnp.maximum(jnp.abs(jnp.sum(query * new_norm, axis=-1, keepdims=True)), 1.0)
            mine[:, h * dk:(h + 1) * dk] = (numer / denom * jax.nn.sigmoid(outgate)).astype(BF16)
            updates.append((keep, ak, value, new_stab, new_norm))
        to = [(od, ot) for ot in reversed(range(m if fast else 1)) for od in range(n) if (od, ot) != (0, 0)]
        copies = [
            send(mine, mine, gs_sem.at[b, ot * n + od], gr_sem.at[b, ot * n + od], at(od, ot)) for od, ot in to
        ]
        if fast:
            if b + 1 == last:
                early = spread(last, range(1, m, 2))
            relayed[b] += relay(b, pending[b])
        for h, (keep, ak, value, new_stab, new_norm) in enumerate(updates):
            stab_out[b, h:h + 1, :] = jnp.sum(jnp.where(diagonal, new_stab, 0.0), axis=0, keepdims=True)
            norm_out[b, :, h * dk:(h + 1) * dk] = new_norm
            ak_t = ak.T
            kept = jnp.broadcast_to(keep, (own, dk))
            for s in range(own):
                memory_out[b, s, h] = kept[s:s + 1, :] * mem_v[b, s, h] + ak_t[:, s:s + 1] * value[s:s + 1, :]
        loads["mix", b].wait()
        for c in copies + relayed[b]:
            c.wait_recv()
        if fast:
            every = jnp.concatenate([gated_v[b, t].reshape(n * own, width) for t in range(m)], axis=1)
        if fast and b == last:
            mixed = jnp.dot(every, mix_v[...].reshape(m * width, feats), preferred_element_type=F32)
            x_out[...] = (xf_v[...] + mixed).astype(BF16)
        elif fast:
            mixed = jnp.dot(every, mixcol_v[b].reshape(m * width, cols), preferred_element_type=F32)
            own_cols = xf_v[:, pl.ds(pl.multiple_of(tp * cols, cols), cols)]
            xcol_v[b, tp] = (own_cols + mixed).astype(BF16)
            ref = xcol_v.at[b, tp]
            copies = [send(ref, ref, xs_sem.at[b, o - 1], xr_sem.at[b, o - 1], at(0, o)) for o in range(1, m)]
            if b + 1 == last:
                pending[last] = spread(last, range(2, m, 2))
                relayed[last] += relay(last, early)
            else:
                pending[b + 1] = spread(b + 1, range(1, m))
            for c in copies:
                c.wait_recv()
            for j in range(m):
                xf_v[:, j * cols:(j + 1) * cols] = xcol_v[b, j].astype(F32)
        else:
            every = gated_v[b, 0].reshape(n * own, width)
            mixed = jnp.dot(every, mix_v[b], preferred_element_type=F32)
            for j in range(m):
                piece = mixed[j * rows:(j + 1) * rows, :]
                mix_send[b, j] = piece.astype(BF16)
                mix_own[j] = piece
                xrow_v[j] = xf_v[j * rows:(j + 1) * rows, :].astype(BF16)
            copies = [
                send(mix_send.at[b, lax.rem(tp + o, m)], mix_recv.at[b, o - 1],
                     ms_sem.at[b, o - 1], mr_sem.at[b, o - 1], at(0, o))
                for o in range(1, m)
            ]
            total = mix_own[tp]
            for o, c in enumerate(copies):
                c.wait_recv()
                total = total + mix_recv[b, o].astype(F32)
            xcol_v[b, tp] = (xrow_v[tp].astype(F32) + total).astype(BF16)
            ref = xcol_v.at[b, tp]
            copies = [send(ref, ref, xs_sem.at[b, o - 1], xr_sem.at[b, o - 1], at(0, o)) for o in range(1, m)]
            for c in copies:
                c.wait_recv()
            for j in range(m):
                xf_v[j * rows:(j + 1) * rows, :] = xcol_v[b, j].astype(F32)
            if b == last:
                x_out[...] = xf_v[...].astype(BF16)
    for c in sent:
        c.wait_send()


def store_kernel(*refs):
    count = (len(refs) - 1) // 2
    sources, results, sem = refs[:count], refs[count:2 * count], refs[-1]
    copies = [pltpu.make_async_copy(a, z, sem.at[k]) for k, (a, z) in enumerate(zip(sources, results))]
    for c in copies:
        c.start()
    for c in copies:
        c.wait()


def shards(sizes, tokens, norm_gain, w_query, w_key, w_value, w_outgate, gate_weight, forget_bias, w_mix, memory, normalizer, stabilizer):
    groups, n, m = sizes
    seqs, feats = tokens.shape
    blocks, own, heads, dk, _ = memory.shape
    width = heads * dk
    rows, cols = seqs // m, feats // m
    wide = 4 * width + 128
    fast = cols % 128 == 0 and width % (16 * groups) == 0 and blocks > 1
    hbm = pl.BlockSpec(memory_space=pltpu.HBM)
    vmem = pl.BlockSpec(memory_space=pltpu.VMEM)
    dma = pltpu.SemaphoreType.DMA
    nd, nt, ng = max(n - 1, 1), max(m - 1, 1), max(groups - 1, 1)
    slow_rows = (1, 8, 128) if fast else (m, rows, feats)
    results = (
        ((seqs, feats), BF16),
        (memory.shape, F32),
        ((blocks, own, width), F32),
        ((blocks, heads, own), F32),
    )
    held = pl.pallas_call(
        functools.partial(step_kernel, sizes, fast),
        out_shape=tuple(pltpu.VMEM(shape, kind) for shape, kind in results),
        in_specs=[hbm] * 11 + [pl.BlockSpec(memory_space=pltpu.SMEM)],
        out_specs=(vmem,) * 4,
        scratch_shapes=[
            pltpu.VMEM(norm_gain.shape, F32),
            pltpu.VMEM((blocks, feats, 4 * width), BF16),
            pltpu.VMEM((blocks, heads, 2, 3 * dk), BF16),
            pltpu.VMEM((m, width, feats) if fast else w_mix.shape, BF16),
            pltpu.VMEM((blocks - 1, m, width, cols) if fast else (1, 1, 16, 128), BF16),
            pltpu.VMEM(memory.shape, F32),
            pltpu.VMEM((blocks, own, width), F32),
            pltpu.VMEM((blocks, heads, own), F32),
            pltpu.VMEM((seqs, feats), BF16),
            pltpu.VMEM((seqs, feats), F32),
            pltpu.VMEM((blocks, n, own, wide), BF16),
            pltpu.VMEM((n, own, wide), F32),
            pltpu.VMEM((blocks, nd, own, wide), BF16),
            pltpu.VMEM((blocks, m if fast else 1, n, own, width), BF16),
            pltpu.VMEM((blocks, m, seqs, cols) if fast else (blocks, m, rows, feats), BF16),
            pltpu.VMEM((blocks,) + slow_rows, BF16),
            pltpu.VMEM(slow_rows, F32),
            pltpu.VMEM((blocks, nt) + slow_rows[1:], BF16),
            pltpu.VMEM(slow_rows, BF16),
            dma((5 + 6 * blocks,)),
            dma((blocks, nd)), dma((blocks, nd)), dma((blocks, n * m)), dma((blocks, n * m)),
            dma((blocks, nt)), dma((blocks, nt)), dma((blocks, nt)), dma((blocks, nt)),
            dma((blocks, nt)), dma((blocks, nt)), dma((blocks, nt, ng)), dma((blocks, nt, ng)),
        ],
        compiler_params=pltpu.CompilerParams(collective_id=0, has_side_effects=True, vmem_limit_bytes=32 << 20),
    )(
        *(
            pltpu.with_memory_space_constraint(t, pltpu.HBM)
            for t in (
                tokens, norm_gain, w_query, w_key, w_value, w_outgate,
                jnp.swapaxes(gate_weight, 2, 3), w_mix, memory, normalizer.reshape(blocks, own, width),
                jnp.swapaxes(stabilizer, 1, 2),
            )
        ),
        forget_bias.T,
    )
    x, new_memory, norm, stab = pl.pallas_call(
        store_kernel,
        out_shape=tuple(jax.ShapeDtypeStruct(shape, kind) for shape, kind in results),
        in_specs=[vmem] * 4,
        out_specs=(pl.BlockSpec(memory_space=pl.ANY),) * 4,
        scratch_shapes=[dma((4,))],
    )(*(pltpu.with_memory_space_constraint(t, pltpu.VMEM) for t in held))
    return x, new_memory, norm.reshape(normalizer.shape), jnp.swapaxes(stab, 1, 2)


def solution(mesh):
    in_specs = (
        P("grp", "dp"),
        P(None, "dp"),
        P(None, "dp", "tp"),
        P(None, "dp", "tp"),
        P(None, "dp", "tp"),
        P(None, "dp", "tp"),
        P(None, "tp", None, None),
        P(None, "tp"),
        P(None, "tp", "dp"),
        P(None, ("grp", "dp"), "tp", None, None),
        P(None, ("grp", "dp"), "tp", None),
        P(None, ("grp", "dp"), "tp"),
    )
    out_specs = (
        P("grp", "dp"),
        P(None, ("grp", "dp"), "tp", None, None),
        P(None, ("grp", "dp"), "tp", None),
        P(None, ("grp", "dp"), "tp"),
    )
    body = functools.partial(shards, (mesh.shape["grp"], mesh.shape["dp"], mesh.shape["tp"]))
    return jax.shard_map(body, mesh=mesh, in_specs=in_specs, out_specs=out_specs, check_vma=False)
```

time: 41.5 us -> 38.2 us (0.920)
  Pallas kernels: 40.7 us -> 36.7 us
  local copies, waits for them, and re-layouts: 0 us -> 0.65 us
    pallas_call x2, Pallas kernels: 40.7 us -> 36.7 us  [the longest x1 35.3 us: shards(): pl.pallas_call(functools.partial(step_kernel, sizes, fast), out_shape=tup...]
    unnamed x0 -> x2, local copies, waits for them, and re-layouts: none -> 0.65 us
where the time goes in v3:
time: 38.2 us; the launch traced here: 38 us
  Pallas kernels  36.7 us (96%)
  local copies, waits for them, and re-layouts  0.65 us (2%)
  between operations  0.65 us (2%)
    pallas_call x1, Pallas kernels, shards(): pl.pallas_call(functools.partial(step_kernel, sizes, fast), out_shape=tup...  35.3 us
    pallas_call x1, Pallas kernels, shards(): pl.pallas_call(store_kernel, out_shape=tuple((jax.ShapeDtypeStruct(shape,...  1.4 us

profile of v3, /device:TPU:0, one launch (start us, length us, event | category | flops | bytes accessed | tf_op | source)
XLA Modules:
  0.0 38.0 jit_solution(5264585445004370078)
XLA Ops:
  0.6 0.0 copy-start
  0.6 0.6 %copy-done = f32[2,1]{0,1:T(1,128)S(1)} copy-done((f32[2,1]{0,1:T(1,128)S(1)}, f32[2,1]{0,1:T(1,128)}, u32[]{:S(2)}) %copy-start) | copy-done | bytes 32
  1.3 35.3 %shard_map.147 = (bf16[64,1024]{1,0:T(8,128)(2,1)S(1)}, f32[2,16,1,128,128]{4,3,2,1,0:T(8,128)S(1)}, f32[2,16,128]{2,1,0:T(8,128)S(1)}, f32[2,1,16]{2,1,0:T(1,128)S(1)}) custom-call(bf16[64,1024]{1,0:T(8,128)(2,1)} %tokens.1, f32[2,1024]{1,0:T(2,128)} %gain.1, bf16[2,1024,128]{2,1,0:T(8,128)(2,1)} %w_query.1, bf16[2,1024,128]{2,1,0:T(8,128)(2,1)} %w_key.1, ...), custom_call_target="tpu_custom_call" | custom-call | tf_op jit(solution)/shard_map/pallas_call | solution.py:275
  36.6 1.4 %shard_map.148 = (bf16[64,1024]{1,0:T(8,128)(2,1)}, f32[2,16,1,128,128]{4,3,2,1,0:T(8,128)}, f32[2,16,128]{2,1,0:T(8,128)}, f32[2,1,16]{2,1,0:T(1,128)}) custom-call(bf16[64,1024]{1,0:T(8,128)(2,1)S(1)} %get-tuple-element.12.refs_0_, f32[2,16,1,128,128]{4,3,2,1,0:T(8,128)S(1)} %get-tuple-element.13.refs_1_, f32[2,16,128]{2,1,0:T(8,128)S(1)} %get-tuple-element.14.refs_2_, ...), custom_call_target="tpu_custom_call" | custom-call | tf_op jit(solution)/shard_map/pallas_call | solution.py:317
Async XLA Ops:
  0.6 0.7 %copy-start = (f32[2,1]{0,1:T(1,128)S(1)}, f32[2,1]{0,1:T(1,128)}, u32[]{:S(2)}) copy-start(f32[2,1]{0,1:T(1,128)} %param.19) | copy-start | bytes 28

commit v4 on v3

--- a/solution.py
+++ b/solution.py
@@ -15,9 +15,9 @@
 
 def step_kernel(
     sizes, fast,
-    tokens, gain, w_query, w_key, w_value, w_outgate, gate_w, w_mix, memory, normalizer, stabilizer, bias,
+    tokens, gain, w_query, w_key, w_value, w_outgate, gate_w, w_mix, memory, normalizer, stabilizer, bias_h,
     x_out, memory_out, norm_out, stab_out,
-    gain_v, w_v, gate_v, mix_v, mixcol_v, mem_v, norm_v, stab_v, tokens_v, xf_v, part_send, part_own, part_recv,
+    gain_v, w_v, gate_v, mix_v, mixcol_v, mem_v, norm_v, stab_v, bias, tokens_v, xf_v, part_send, part_own, part_recv,
     gated_v, xcol_v, mix_send, mix_own, mix_recv, xrow_v,
     load_sem, ps_sem, pr_sem, gs_sem, gr_sem, ms_sem, mr_sem, xs_sem, xr_sem, zs_sem, zr_sem, ys_sem, yr_sem,
 ):
@@ -46,6 +46,7 @@
             order.append(("gate", 0, gate_w, gate_v))
             order.append(("norm", 0, normalizer, norm_v))
             order.append(("stab", 0, stabilizer, stab_v))
+            order.append(("bias", 0, bias_h, bias))
         order.append(("mem", b, memory.at[b], mem_v.at[b]))
         if fast:
             order.append(("mix", b, w_mix.at[b, :, mix_cols(b, tp)], mix_slot(b, tp)))
@@ -136,6 +137,7 @@
             loads["gate", 0].wait()
             loads["norm", 0].wait()
             loads["stab", 0].wait()
+            loads["bias", 0].wait()
         loads["mem", b].wait()
         total = part_own[dp]
         for o, c in enumerate(copies):
@@ -206,11 +208,12 @@
             copies = [send(ref, ref, xs_sem.at[b, o - 1], xr_sem.at[b, o - 1], at(0, o)) for o in range(1, m)]
             if b + 1 == last:
                 pending[last] = spread(last, range(2, m, 2))
-                relayed[last] += relay(last, early)
             else:
                 pending[b + 1] = spread(b + 1, range(1, m))
             for c in copies:
                 c.wait_recv()
+            if b + 1 == last:
+                relayed[last] += relay(last, early)
             for j in range(m):
                 xf_v[:, j * cols:(j + 1) * cols] = xcol_v[b, j].astype(F32)
         else:
@@ -275,7 +278,7 @@
     held = pl.pallas_call(
         functools.partial(step_kernel, sizes, fast),
         out_shape=tuple(pltpu.VMEM(shape, kind) for shape, kind in results),
-        in_specs=[hbm] * 11 + [pl.BlockSpec(memory_space=pltpu.SMEM)],
+        in_specs=[hbm] * 12,
         out_specs=(vmem,) * 4,
         scratch_shapes=[
             pltpu.VMEM(norm_gain.shape, F32),
@@ -286,6 +289,7 @@
             pltpu.VMEM(memory.shape, F32),
             pltpu.VMEM((blocks, own, width), F32),
             pltpu.VMEM((blocks, heads, own), F32),
+            pltpu.SMEM((heads, blocks), F32),
             pltpu.VMEM((seqs, feats), BF16),
             pltpu.VMEM((seqs, feats), F32),
             pltpu.VMEM((blocks, n, own, wide), BF16),
@@ -297,7 +301,7 @@
             pltpu.VMEM(slow_rows, F32),
             pltpu.VMEM((blocks, nt) + slow_rows[1:], BF16),
             pltpu.VMEM(slow_rows, BF16),
-            dma((5 + 6 * blocks,)),
+            dma((6 + 6 * blocks,)),
             dma((blocks, nd)), dma((blocks, nd)), dma((blocks, n * m)), dma((blocks, n * m)),
             dma((blocks, nt)), dma((blocks, nt)), dma((blocks, nt)), dma((blocks, nt)),
             dma((blocks, nt)), dma((blocks, nt)), dma((blocks, nt, ng)), dma((blocks, nt, ng)),
@@ -309,10 +313,9 @@
             for t in (
                 tokens, norm_gain, w_query, w_key, w_value, w_outgate,
                 jnp.swapaxes(gate_weight, 2, 3), w_mix, memory, normalizer.reshape(blocks, own, width),
-                jnp.swapaxes(stabilizer, 1, 2),
+                jnp.swapaxes(stabilizer, 1, 2), forget_bias.T,
             )
         ),
-        forget_bias.T,
     )
     x, new_memory, norm, stab = pl.pallas_call(
         store_kernel,

time: 38.2 us -> 37 us (0.969)
  local copies, waits for them, and re-layouts: 0.65 us -> 0 us
  Pallas kernels: 36.7 us -> 36.2 us
    unnamed x2 -> x0, local copies, waits for them, and re-layouts: 0.65 us -> none
    pallas_call x1, Pallas kernels: 35.3 us -> 34.8 us  [shards(): pl.pallas_call(functools.partial(step_kernel, sizes, fast), out_shape=tup...]
where the time goes in v4:
time: 37 us; the launch traced here: 36.9 us
  Pallas kernels  36.2 us (98%)
  between operations  0.64 us (2%)
    pallas_call x1, Pallas kernels, shards(): pl.pallas_call(functools.partial(step_kernel, sizes, fast), out_shape=tup...  34.8 us
    pallas_call x1, Pallas kernels, shards(): pl.pallas_call(store_kernel, out_shape=tuple((jax.ShapeDtypeStruct(shape,...  1.4 us

profile of v4, /device:TPU:0, one launch (start us, length us, event | category | flops | bytes accessed | tf_op | source)
XLA Modules:
  0.0 36.9 jit_solution(8924612505257034135)
XLA Ops:
  0.6 34.8 %shard_map.147 = (bf16[64,1024]{1,0:T(8,128)(2,1)S(1)}, f32[2,16,1,128,128]{4,3,2,1,0:T(8,128)S(1)}, f32[2,16,128]{2,1,0:T(8,128)S(1)}, f32[2,1,16]{2,1,0:T(1,128)S(1)}) custom-call(bf16[64,1024]{1,0:T(8,128)(2,1)} %tokens.1, f32[2,1024]{1,0:T(2,128)} %gain.1, bf16[2,1024,128]{2,1,0:T(8,128)(2,1)} %w_query.1, bf16[2,1024,128]{2,1,0:T(8,128)(2,1)} %w_key.1, ...), custom_call_target="tpu_custom_call" | custom-call | tf_op jit(solution)/shard_map/pallas_call | solution.py:278
  35.5 1.4 %shard_map.148 = (bf16[64,1024]{1,0:T(8,128)(2,1)}, f32[2,16,1,128,128]{4,3,2,1,0:T(8,128)}, f32[2,16,128]{2,1,0:T(8,128)}, f32[2,1,16]{2,1,0:T(1,128)}) custom-call(bf16[64,1024]{1,0:T(8,128)(2,1)S(1)} %get-tuple-element.12.refs_0_, f32[2,16,1,128,128]{4,3,2,1,0:T(8,128)S(1)} %get-tuple-element.13.refs_1_, f32[2,16,128]{2,1,0:T(8,128)S(1)} %get-tuple-element.14.refs_2_, ...), custom_call_target="tpu_custom_call" | custom-call | tf_op jit(solution)/shard_map/pallas_call | solution.py:320

commit v5 on v4

--- a/solution.py
+++ b/solution.py
@@ -33,10 +33,10 @@
     last = blocks - 1
 
     def mix_slot(b, t):
-        return mix_v.at[t] if b == last else mixcol_v.at[b, t]
+        return mixcol_v.at[b, t]
 
     def mix_cols(b, to):
-        return pl.ds(0, feats) if b == last else pl.ds(pl.multiple_of(to * cols, cols), cols)
+        return pl.ds(pl.multiple_of(to * cols, cols), cols)
 
     order = [("x", 0, tokens, tokens_v), ("g", 0, gain, gain_v)]
     for b in range(blocks):
@@ -182,9 +182,9 @@
             send(mine, mine, gs_sem.at[b, ot * n + od], gr_sem.at[b, ot * n + od], at(od, ot)) for od, ot in to
         ]
         if fast:
-            if b + 1 == last:
-                early = spread(last, range(1, m, 2))
             relayed[b] += relay(b, pending[b])
+            if b < last:
+                pending[b + 1] = spread(b + 1, range(1, m))
         for h, (keep, ak, value, new_stab, new_norm) in enumerate(updates):
             stab_out[b, h:h + 1, :] = jnp.sum(jnp.where(diagonal, new_stab, 0.0), axis=0, keepdims=True)
             norm_out[b, :, h * dk:(h + 1) * dk] = new_norm
@@ -197,25 +197,19 @@
             c.wait_recv()
         if fast:
             every = jnp.concatenate([gated_v[b, t].reshape(n * own, width) for t in range(m)], axis=1)
-        if fast and b == last:
-            mixed = jnp.dot(every, mix_v[...].reshape(m * width, feats), preferred_element_type=F32)
-            x_out[...] = (xf_v[...] + mixed).astype(BF16)
-        elif fast:
+        if fast:
             mixed = jnp.dot(every, mixcol_v[b].reshape(m * width, cols), preferred_element_type=F32)
             own_cols = xf_v[:, pl.ds(pl.multiple_of(tp * cols, cols), cols)]
             xcol_v[b, tp] = (own_cols + mixed).astype(BF16)
             ref = xcol_v.at[b, tp]
             copies = [send(ref, ref, xs_sem.at[b, o - 1], xr_sem.at[b, o - 1], at(0, o)) for o in range(1, m)]
-            if b + 1 == last:
-                pending[last] = spread(last, range(2, m, 2))
-            else:
-                pending[b + 1] = spread(b + 1, range(1, m))
             for c in copies:
                 c.wait_recv()
-            if b + 1 == last:
-                relayed[last] += relay(last, early)
             for j in range(m):
-                xf_v[:, j * cols:(j + 1) * cols] = xcol_v[b, j].astype(F32)
+                if b == last:
+                    x_out[:, j * cols:(j + 1) * cols] = xcol_v[b, j]
+                else:
+                    xf_v[:, j * cols:(j + 1) * cols] = xcol_v[b, j].astype(F32)
         else:
             every = gated_v[b, 0].reshape(n * own, width)
             mixed = jnp.dot(every, mix_v[b], preferred_element_type=F32)
@@ -263,7 +257,7 @@
     width = heads * dk
     rows, cols = seqs // m, feats // m
     wide = 4 * width + 128
-    fast = cols % 128 == 0 and width % (16 * groups) == 0 and blocks > 1
+    fast = cols % 128 == 0 and width % (16 * groups) == 0
     hbm = pl.BlockSpec(memory_space=pltpu.HBM)
     vmem = pl.BlockSpec(memory_space=pltpu.VMEM)
     dma = pltpu.SemaphoreType.DMA
@@ -284,8 +278,8 @@
             pltpu.VMEM(norm_gain.shape, F32),
             pltpu.VMEM((blocks, feats, 4 * width), BF16),
             pltpu.VMEM((blocks, heads, 2, 3 * dk), BF16),
-            pltpu.VMEM((m, width, feats) if fast else w_mix.shape, BF16),
-            pltpu.VMEM((blocks - 1, m, width, cols) if fast else (1, 1, 16, 128), BF16),
+            pltpu.VMEM((1, 16, 128) if fast else w_mix.shape, BF16),
+            pltpu.VMEM((blocks, m, width, cols) if fast else (1, 1, 16, 128), BF16),
             pltpu.VMEM(memory.shape, F32),
             pltpu.VMEM((blocks, own, width), F32),
             pltpu.VMEM((blocks, heads, own), F32),

time: 37 us -> 35 us (0.946)
  Pallas kernels: 36.2 us -> 34.2 us
    pallas_call x1, Pallas kernels: 34.8 us -> 32.8 us  [shards(): pl.pallas_call(functools.partial(step_kernel, sizes, fast), out_shape=tup...]
where the time goes in v5:
time: 35 us; the launch traced here: 34.8 us
  Pallas kernels  34.2 us (98%)
  between operations  0.64 us (2%)
    pallas_call x1, Pallas kernels, shards(): pl.pallas_call(functools.partial(step_kernel, sizes, fast), out_shape=tup...  32.8 us
    pallas_call x1, Pallas kernels, shards(): pl.pallas_call(store_kernel, out_shape=tuple((jax.ShapeDtypeStruct(shape,...  1.4 us

profile of v5, /device:TPU:0, one launch (start us, length us, event | category | flops | bytes accessed | tf_op | source)
XLA Modules:
  0.0 34.8 jit_solution(10550607216148828790)
XLA Ops:
  0.6 32.8 %shard_map.147 = (bf16[64,1024]{1,0:T(8,128)(2,1)S(1)}, f32[2,16,1,128,128]{4,3,2,1,0:T(8,128)S(1)}, f32[2,16,128]{2,1,0:T(8,128)S(1)}, f32[2,1,16]{2,1,0:T(1,128)S(1)}) custom-call(bf16[64,1024]{1,0:T(8,128)(2,1)} %tokens.1, f32[2,1024]{1,0:T(2,128)} %gain.1, bf16[2,1024,128]{2,1,0:T(8,128)(2,1)} %w_query.1, bf16[2,1024,128]{2,1,0:T(8,128)(2,1)} %w_key.1, ...), custom_call_target="tpu_custom_call" | custom-call | tf_op jit(solution)/shard_map/pallas_call | solution.py:272
  33.4 1.4 %shard_map.148 = (bf16[64,1024]{1,0:T(8,128)(2,1)}, f32[2,16,1,128,128]{4,3,2,1,0:T(8,128)}, f32[2,16,128]{2,1,0:T(8,128)}, f32[2,1,16]{2,1,0:T(1,128)}) custom-call(bf16[64,1024]{1,0:T(8,128)(2,1)S(1)} %get-tuple-element.12.refs_0_, f32[2,16,1,128,128]{4,3,2,1,0:T(8,128)S(1)} %get-tuple-element.13.refs_1_, f32[2,16,128]{2,1,0:T(8,128)S(1)} %get-tuple-element.14.refs_2_, ...), custom_call_target="tpu_custom_call" | custom-call | tf_op jit(solution)/shard_map/pallas_call | solution.py:314

commit v6 on v5

--- a/solution.py
+++ b/solution.py
@@ -109,16 +109,30 @@
     loads["g", 0].wait()
     xf_v[...] = tokens_v[...].astype(F32)
     for b in range(blocks):
-        xf = xf_v[...]
-        squares = jnp.sum(xf * xf, axis=-1, keepdims=True)
-        scaled_in = (xf * gain_v[b:b + 1, :]).astype(BF16)
+        by_piece = fast and b > 0
+        if not by_piece:
+            xf = xf_v[...]
+            squares = jnp.sum(xf * xf, axis=-1, keepdims=True)
+            scaled_in = (xf * gain_v[b:b + 1, :]).astype(BF16)
         if b == 0:
             pl.semaphore_wait(barrier, greeted)
             if fast:
                 pending[0] = spread(0, range(1, m))
         for k in range(4):
             loads[f"w{k}", b].wait()
-        part = jnp.dot(scaled_in, w_v[b], preferred_element_type=F32)
+        if by_piece:
+            for o in range(m):
+                if o:
+                    arriving[o - 1].wait_recv()
+                frm = lax.rem(tp + m - o, m)
+                where = pl.ds(pl.multiple_of(frm * cols, cols), cols)
+                xf = xcol_v[b - 1, frm].astype(F32)
+                square = jnp.sum(xf * xf, axis=-1, keepdims=True)
+                scaled_in = (xf * gain_v[b:b + 1, where]).astype(BF16)
+                term = jnp.dot(scaled_in, w_v[b, where, :], preferred_element_type=F32)
+                part, squares = (part + term, squares + square) if o else (term, square)
+        else:
+            part = jnp.dot(scaled_in, w_v[b], preferred_element_type=F32)
         for j in range(n):
             piece = part[j * own:(j + 1) * own, :]
             sq = jnp.broadcast_to(squares[j * own:(j + 1) * own, :], (own, 128))
@@ -199,17 +213,19 @@
             every = jnp.concatenate([gated_v[b, t].reshape(n * own, width) for t in range(m)], axis=1)
         if fast:
             mixed = jnp.dot(every, mixcol_v[b].reshape(m * width, cols), preferred_element_type=F32)
-            own_cols = xf_v[:, pl.ds(pl.multiple_of(tp * cols, cols), cols)]
+            if b == 0:
+                own_cols = xf_v[:, pl.ds(pl.multiple_of(tp * cols, cols), cols)]
+            else:
+                own_cols = xcol_v[b - 1, tp].astype(F32)
             xcol_v[b, tp] = (own_cols + mixed).astype(BF16)
             ref = xcol_v.at[b, tp]
             copies = [send(ref, ref, xs_sem.at[b, o - 1], xr_sem.at[b, o - 1], at(0, o)) for o in range(1, m)]
-            for c in copies:
-                c.wait_recv()
-            for j in range(m):
-                if b == last:
+            arriving = copies
+            if b == last:
+                for c in copies:
+                    c.wait_recv()
+                for j in range(m):
                     x_out[:, j * cols:(j + 1) * cols] = xcol_v[b, j]
-                else:
-                    xf_v[:, j * cols:(j + 1) * cols] = xcol_v[b, j].astype(F32)
         else:
             every = gated_v[b, 0].reshape(n * own, width)
             mixed = jnp.dot(every, mix_v[b], preferred_element_type=F32)

time: 35 us -> 34.9 us (level)
  no operation moved by 1% of the time
where the time goes in v6:
time: 34.9 us; the launch traced here: 34.7 us
  Pallas kernels  34.1 us (98%)
  between operations  0.64 us (2%)
    pallas_call x1, Pallas kernels, shards(): pl.pallas_call(functools.partial(step_kernel, sizes, fast), out_shape=tup...  32.7 us
    pallas_call x1, Pallas kernels, shards(): pl.pallas_call(store_kernel, out_shape=tuple((jax.ShapeDtypeStruct(shape,...  1.4 us

profile of v6, /device:TPU:0, one launch (start us, length us, event | category | flops | bytes accessed | tf_op | source)
XLA Modules:
  0.0 34.7 jit_solution(12104067811895912500)
XLA Ops:
  0.6 32.7 %shard_map.147 = (bf16[64,1024]{1,0:T(8,128)(2,1)S(1)}, f32[2,16,1,128,128]{4,3,2,1,0:T(8,128)S(1)}, f32[2,16,128]{2,1,0:T(8,128)S(1)}, f32[2,1,16]{2,1,0:T(1,128)S(1)}) custom-call(bf16[64,1024]{1,0:T(8,128)(2,1)} %tokens.1, f32[2,1024]{1,0:T(2,128)} %gain.1, bf16[2,1024,128]{2,1,0:T(8,128)(2,1)} %w_query.1, bf16[2,1024,128]{2,1,0:T(8,128)(2,1)} %w_key.1, ...), custom_call_target="tpu_custom_call" | custom-call | tf_op jit(solution)/shard_map/pallas_call | solution.py:288
  33.3 1.4 %shard_map.148 = (bf16[64,1024]{1,0:T(8,128)(2,1)}, f32[2,16,1,128,128]{4,3,2,1,0:T(8,128)}, f32[2,16,128]{2,1,0:T(8,128)}, f32[2,1,16]{2,1,0:T(1,128)}) custom-call(bf16[64,1024]{1,0:T(8,128)(2,1)S(1)} %get-tuple-element.12.refs_0_, f32[2,16,1,128,128]{4,3,2,1,0:T(8,128)S(1)} %get-tuple-element.13.refs_1_, f32[2,16,128]{2,1,0:T(8,128)S(1)} %get-tuple-element.14.refs_2_, ...), custom_call_target="tpu_custom_call" | custom-call | tf_op jit(solution)/shard_map/pallas_call | solution.py:330
